TPU v7x, 256 devices: a 2x2x32 block of a 4x16x32 slice. The times are simulated.
256 devices in a mesh: grp: 4 (over y, x), ep: 32 (over z), tp: 2 (over core).
Axes of the slice: x: 2, y: 2, z: 32, core: 2. Of those that a mesh axis runs over, the one named last changes fastest.
The devices are a block of a 4x16x32 slice.
Arguments:
- tokens: bfloat16 [8192, 2048], P(('grp', 'ep')), parts along dimension 0, may hold values from -6 to 6
- routes: int32 [8192, 4], P(('grp', 'ep')), parts along dimension 0, may hold values from 0 to 31, all different within a row; in each aligned block of 64 rows (0 to 63, 64 to 127, ...) at most 16 rows name the same one
- gate_weights: float32 [8192, 4], P(('grp', 'ep')), parts along dimension 0, may hold values from 0.05 to 1
- w_gate: bfloat16 [32, 2048, 1280], P('ep', None, 'tp'), may hold values from -0.125 to 0.125
- w_up: bfloat16 [32, 2048, 1280], P('ep', None, 'tp'), may hold values from -0.125 to 0.125
- w_down: bfloat16 [32, 1280, 2048], P('ep', 'tp'), may hold values from -0.15625 to 0.15625
- norm_gain: float32 [2048], P('tp'), may hold values from 0.1 to 1.9
- norm_bias: float32 [2048], P('tp'), may hold values from -2 to 2
Outputs:
- normed: bfloat16 [8192, 2048], P(('grp', 'ep'), 'tp'), parts along dimension 0
There are 4 independent parts, one for each index of `grp`. A program takes and returns all parts, laid end to end along the dimension named above; an argument that names none is the same for every part. Nothing has to cross between parts.
Inputs may be any that keep to these rules, and one draw needn't show every extreme that they name: `routes`: the rows of a token name distinct experts; in each aligned block of 64 rows (the tokens of one index of ep) no expert is named more than 16 times, a bound that some block reaches.
All inputs are finite; a program needn't handle non-finite values.
Results may differ from a plain program's by a relative error of at most 0.0037.
Values may be sent and summed in bfloat16 or wider, within the bound.
A program may use at most 64 MiB of HBM per device.

v0:
```python
import jax
import jax.numpy as jnp
from jax import lax
from jax.sharding import PartitionSpec as P

residual_scale = 1.4142135
norm_eps = 1e-05


def in_order(blocks, dim):
    lengths = list(blocks.shape[1:])
    lengths[dim] *= blocks.shape[0]
    return jnp.moveaxis(blocks, 0, dim).reshape(lengths)


def from_everyone(array, axis):
    copies = jnp.broadcast_to(array, (lax.axis_size(axis), *array.shape))
    return lax.all_to_all(copies, axis, split_axis=0, concat_axis=0, tiled=True)


def collect(array, axis, dim):
    return in_order(from_everyone(array, axis), dim)


def split_up(array, dim, size):
    lengths = array.shape
    blocks = array.reshape(*lengths[:dim], size, lengths[dim] // size, *lengths[dim + 1 :])
    return jnp.moveaxis(blocks, dim, 0)


def sum_at_owner(array, axis, dim):
    size = lax.axis_size(axis)
    blocks = lax.all_to_all(split_up(array, dim, size), axis, 0, 0, tiled=True)
    return jnp.sum(blocks.astype(jnp.float32), axis=0)


def shards(tokens, routes, gate_weights, w_gate, w_up, w_down, norm_gain, norm_bias):
    num_ep = lax.axis_size("ep")
    num_tp = lax.axis_size("tp")
    tp_index = lax.axis_index("tp")
    tok_rows, width = tokens.shape
    top_count = routes.shape[1]
    experts = num_ep * w_gate.shape[0]
    capacity = 2 * tok_rows * top_count // experts
    half_width = width // num_tp
    pair_list = routes.reshape(-1)
    onehot = (pair_list[:, None] == jnp.arange(experts, dtype=jnp.int32)).astype(jnp.int32)
    slots = jnp.sum((jnp.cumsum(onehot, axis=0) - onehot) * onehot, axis=1)
    target = pair_list * capacity + slots
    placing = jnp.arange(experts * capacity, dtype=jnp.int32)[:, None] == target[None, :]
    placing = jnp.sum(
        placing.reshape(experts * capacity, tok_rows, top_count).astype(jnp.float32), axis=2
    )
    placing = placing.astype(jnp.bfloat16)
    own_half = lax.dynamic_slice_in_dim(tokens, tp_index * half_width, half_width, 1)
    outgoing = jnp.dot(placing, own_half, preferred_element_type=jnp.float32).astype(jnp.bfloat16)
    arrived = lax.all_to_all(outgoing, "ep", split_axis=0, concat_axis=0, tiled=True)
    received = collect(arrived, "tp", 1)
    gate = jnp.dot(received, w_gate[0], preferred_element_type=jnp.float32)
    upper = jnp.dot(received, w_up[0], preferred_element_type=jnp.float32)
    hidden = (jax.nn.silu(gate) * upper).astype(jnp.bfloat16)
    partial_sum = jnp.dot(hidden, w_down[0], preferred_element_type=jnp.float32).astype(
        jnp.bfloat16
    )
    expert_out = sum_at_owner(partial_sum, "tp", 1).astype(jnp.bfloat16)
    came_back = lax.all_to_all(expert_out, "ep", split_axis=0, concat_axis=0, tiled=True)
    chosen = came_back[target].astype(jnp.float32).reshape(tok_rows, top_count, half_width)
    mixture = jnp.sum(gate_weights[:, :, None] * chosen, axis=1).astype(jnp.bfloat16)
    own_tokens = lax.dynamic_slice_in_dim(tokens, tp_index * half_width, half_width, 1)
    summed = residual_scale * own_tokens.astype(jnp.float32) + mixture.astype(jnp.float32)
    row_sum, row_squares = lax.psum(
        (jnp.sum(summed, axis=1), jnp.sum(summed * summed, axis=1)), "tp"
    )
    mean = row_sum / width
    variance = row_squares / width - mean * mean
    normed = (summed - mean[:, None]) * lax.rsqrt(
        variance[:, None] + norm_eps
    ) * norm_gain + norm_bias
    return normed.astype(jnp.bfloat16)


def solution(mesh):
    in_specs = (
        P(("grp", "ep"), None),
        P(("grp", "ep"), None),
        P(("grp", "ep"), None),
        P("ep", None, "tp"),
        P("ep", None, "tp"),
        P("ep", "tp", None),
        P("tp"),
        P("tp"),
    )
    out_specs = P(("grp", "ep"), "tp")
    return jax.shard_map(shards, mesh=mesh, in_specs=in_specs, out_specs=out_specs, check_vma=False)
```

profile of v0, /device:TPU:37, one launch (start us, length us, event | category | flops | bytes accessed | tf_op | source)
XLA Modules:
  0.0 297.8 jit_solution(14020260408673805681)
XLA Ops:
  0.0 0.0 copy-start
  0.0 0.9 copy.25
  0.9 0.1 eq.44
  1.0 0.1 eq.40
  1.2 0.6 reduce-window.6
  1.7 0.2 slice_reduce_fusion
  2.0 0.1 fusion.19
  2.1 0.1 reduce_sum.62
  2.2 0.1 copy.29
  2.3 0.1 convert_reduce_fusion
  2.4 1.4 convolution_convert_fusion.1
  3.8 137.5 %all_to_all.34 = bf16[32,16,1024]{2,1,0:T(8,128)(2,1)} all-to-all(bf16[32,16,1024]{2,1,0:T(8,128)(2,1)S(1)} %bitcast.55), channel_id=1, replica_groups=mesh['grp'=4,'ep'=32,'tp'=2] {'ep'}, dimensions={0} | all-to-all | bytes 2097152 | tf_op jit(solution)/shard_map/all_to_all | solution.py:57
  141.3 2.3 copy.30
  143.6 1.4 broadcast_in_dim.2
  145.0 0.0 copy-start.6
  145.0 6.3 %all_to_all.35 = bf16[2,512,1024]{1,2,0:T(8,128)(2,1)S(1)} all-to-all(bf16[2,512,1024]{1,2,0:T(8,128)(2,1)S(1)} %broadcast_in_dim.2), channel_id=1, replica_groups=mesh['grp'=4,'ep'=32,'tp'=2] {'tp'}, dimensions={0} | all-to-all | bytes 4194304 | tf_op jit(solution)/shard_map/all_to_all | solution.py:18
  151.3 0.0 copy-start.1
  151.3 1.3 copy-done.1
  152.6 0.0 copy-done.6
  152.6 2.9 fusion.3
  155.5 0.0 copy-done
  155.5 8.2 %convolution_convert_fusion = bf16[512,2048]{1,0:T(8,128)(2,1)} fusion(bf16[1,640,2048]{2,1,0:T(8,128)(2,1)S(1)} %copy-done, bf16[512,2048]{0,1:T(8,128)(2,1)} %bitcast.58, bf16[1,2048,640]{2,1,0:T(8,128)(2,1)} %param.12, f32[512,640]{1,0:T(8,128)} %fusion.3), kind=kOutput, calls=%fused_computation.1 | convolution fusion | flops 2687369216 | bytes 10747904 | tf_op jit(solution)/shard_map/dot_general | solution.py:62
  163.7 1.8 copy.36
  165.5 6.3 %all_to_all.36 = bf16[2,512,1024]{2,1,0:T(8,128)(2,1)} all-to-all(bf16[2,512,1024]{2,1,0:T(8,128)(2,1)S(1)} %bitcast.53), channel_id=1, replica_groups=mesh['grp'=4,'ep'=32,'tp'=2] {'tp'}, dimensions={0} | all-to-all | bytes 4194304 | tf_op jit(solution)/shard_map/all_to_all | solution.py:33
  171.8 0.0 copy-start.5
  171.8 3.3 %reduce_sum.64 = bf16[512,1024]{1,0:T(8,128)(2,1)} reduce(bf16[2,512,1024]{2,1,0:T(8,128)(2,1)} %all_to_all.36, bf16[]{:T(256)} %constant.30.clone.1), dimensions={0}, to_apply=%region_4.5 | reduce | flops 524288 | bytes 3145730 | tf_op jit(solution)/shard_map/reduce_sum | solution.py:34
  175.1 7.8 %all-to-all-start.3 = ((bf16[32,16,1024]{2,1,0:T(8,128)(2,1)}), bf16[32,16,1024]{2,1,0:T(8,128)(2,1)}, u32[]{:S(2)}, u32[]{:S(2)}) async-start(bf16[32,16,1024]{2,1,0:T(8,128)(2,1)} %bitcast.54), calls=%async_computation.3 | async-start | bytes 2097152 | tf_op jit(solution)/shard_map/all_to_all | solution.py:66
  183.0 0.1 mul.79
  183.1 0.0 copy-done.5
  183.1 0.1 copy.24
  183.2 104.5 %all-to-all-done.3 = bf16[32,16,1024]{2,1,0:T(8,128)(2,1)} async-done(((bf16[32,16,1024]{2,1,0:T(8,128)(2,1)}), bf16[32,16,1024]{2,1,0:T(8,128)(2,1)}, u32[]{:S(2)}, u32[]{:S(2)}) %all-to-all-start.3) | async-done | bytes 1048608 | tf_op jit(solution)/shard_map/all_to_all | solution.py:66
  287.7 2.9 gather_fusion
  290.6 0.0 copy-start.2
  290.6 0.0 copy-start.3
  290.6 0.0 copy-start.4
  290.7 1.3 reshape.87
  292.0 2.0 multiply_reduce_fusion
  293.9 0.0 copy-done.2
  294.0 0.2 fusion.14
  294.1 2.9 all-reduce
  297.1 0.0 copy-done.3
  297.1 0.0 copy-done.4
  297.1 0.8 add_convert_fusion
  (7 shorter events, 0.1 us)
Async XLA Ops:
  0.0 155.5 %copy-start = (bf16[1,640,2048]{2,1,0:T(8,128)(2,1)S(1)}, bf16[1,640,2048]{2,1,0:T(8,128)(2,1)}, u32[]{:S(2)}) copy-start(bf16[1,640,2048]{2,1,0:T(8,128)(2,1)} %param.13) | copy-start | bytes 7864324
  145.0 7.6 %copy-start.6 = (bf16[1,2048,640]{2,1,0:T(8,128)(2,1)S(1)}, bf16[1,2048,640]{2,1,0:T(8,128)(2,1)}, u32[]{:S(2)}) copy-start(bf16[1,2048,640]{2,1,0:T(8,128)(2,1)} %param.11) | copy-start | bytes 7864324
  151.3 1.4 copy-start.1
  171.8 11.3 %copy-start.5 = (f32[64,4]{0,1:T(4,128)S(1)}, f32[64,4]{0,1:T(4,128)}, u32[]{:S(2)}) copy-start(f32[64,4]{0,1:T(4,128)} %param.10) | copy-start | bytes 3076
  175.1 112.6 %all-to-all-start.3 = ((bf16[32,16,1024]{2,1,0:T(8,128)(2,1)}), bf16[32,16,1024]{2,1,0:T(8,128)(2,1)}, u32[]{:S(2)}, u32[]{:S(2)}) async-start(bf16[32,16,1024]{2,1,0:T(8,128)(2,1)} %bitcast.54), calls=%async_computation.3 | async-start | bytes 2097152 | tf_op jit(solution)/shard_map/all_to_all | solution.py:66
  290.6 3.3 %copy-start.2 = (bf16[64,2048]{1,0:T(8,128)(2,1)S(1)}, bf16[64,2048]{1,0:T(8,128)(2,1)}, u32[]{:S(2)}) copy-start(bf16[64,2048]{1,0:T(8,128)(2,1)} %param.8) | copy-start | bytes 786436
  290.6 6.4 %copy-start.3 = (f32[1024]{0:T(1024)S(1)}, f32[1024]{0:T(1024)}, u32[]{:S(2)}) copy-start(f32[1024]{0:T(1024)} %param.15) | copy-start | bytes 12292
  290.6 6.4 %copy-start.4 = (f32[1024]{0:T(1024)S(1)}, f32[1024]{0:T(1024)}, u32[]{:S(2)}) copy-start(f32[1024]{0:T(1024)} %param.14) | copy-start | bytes 12292
where the time goes:
time: 298 us
  blocking collectives  153 us (51%)
  waiting for transfers between devices  105 us (35%)
  local copies, waits for them, and re-layouts  12.7 us (4%)
  matrix products  12.4 us (4%)
  starting transfers between devices  7.83 us (3%)
  other arithmetic  7.13 us (2%)
    all_to_all x1, blocking collectives, shards(): lax.all_to_all(outgoing, 'ep', split_axis=0, concat_axis=0, tiled=True)  138 us
    all_to_all x1, waiting for transfers between devices, shards(): lax.all_to_all(expert_out, 'ep', split_axis=0, concat_axis=0, tiled=True)  105 us
    dot_general x1, matrix products, shards(): jnp.dot(hidden, w_down[0], preferred_element_type=jnp.float32)  8.15 us
    all_to_all x1, starting transfers between devices, shards(): lax.all_to_all(expert_out, 'ep', split_axis=0, concat_axis=0, tiled=True)  7.83 us
    all_to_all x1, blocking collectives, sum_at_owner(): blocks = lax.all_to_all(split_up(array, dim, size), axis, 0, 0, tiled=True)  6.33 us
    all_to_all x1, blocking collectives, from_everyone(): return lax.all_to_all(copies, axis, split_axis=0, concat_axis=0, tiled=True)  6.26 us
  transfers between devices with their start and end apart: 1, of which 1 were waited for; matrix products, arithmetic and copies ran while one was open for 0% of the time, Pallas kernels for 0%

commit v1 on v0

v1 whole, which is shorter than its diff:
```python
import jax
import jax.numpy as jnp
from jax import lax
from jax.sharding import PartitionSpec as P

residual_scale = 1.4142135
norm_eps = 1e-05


def shards(tokens, routes, gate_weights, w_gate, w_up, w_down, norm_gain, norm_bias):
    tp_index = lax.axis_index("tp")
    ep_index = lax.axis_index("ep")
    num_tp = lax.axis_size("tp")
    tok_rows, width = tokens.shape
    half_width = width // num_tp
    own_half = lax.dynamic_slice_in_dim(tokens, tp_index * half_width, half_width, 1)
    part = lax.all_gather(own_half, "ep", axis=0, tiled=True)
    everyone = lax.all_gather(part, "tp", axis=1, tiled=True)
    all_routes = lax.all_gather(routes, "ep", axis=0, tiled=True)
    all_gates = lax.all_gather(gate_weights, "ep", axis=0, tiled=True)
    weight = jnp.sum(jnp.where(all_routes == ep_index, all_gates, 0.0), axis=1)
    gate = jnp.dot(everyone, w_gate[0], preferred_element_type=jnp.float32)
    upper = jnp.dot(everyone, w_up[0], preferred_element_type=jnp.float32)
    hidden = (jax.nn.silu(gate) * upper).astype(jnp.bfloat16)
    partial_sum = jnp.dot(hidden, w_down[0], preferred_element_type=jnp.float32)
    weighted = (partial_sum * weight[:, None]).astype(jnp.bfloat16)
    mine = lax.psum_scatter(weighted, "tp", scatter_dimension=1, tiled=True)
    mixture = lax.psum_scatter(mine, "ep", scatter_dimension=0, tiled=True)
    summed = residual_scale * own_half.astype(jnp.float32) + mixture.astype(jnp.float32)
    row_sum, row_squares = lax.psum(
        (jnp.sum(summed, axis=1), jnp.sum(summed * summed, axis=1)), "tp"
    )
    mean = row_sum / width
    variance = row_squares / width - mean * mean
    normed = (summed - mean[:, None]) * lax.rsqrt(
        variance[:, None] + norm_eps
    ) * norm_gain + norm_bias
    return normed.astype(jnp.bfloat16)


def solution(mesh):
    in_specs = (
        P(("grp", "ep"), None),
        P(("grp", "ep"), None),
        P(("grp", "ep"), None),
        P("ep", None, "tp"),
        P("ep", None, "tp"),
        P("ep", "tp", None),
        P("tp"),
        P("tp"),
    )
    out_specs = P(("grp", "ep"), "tp")
    return jax.shard_map(shards, mesh=mesh, in_specs=in_specs, out_specs=out_specs, check_vma=False)
```

time: 298 us -> 478 us (1.60)
  waiting for transfers between devices: 105 us -> 326 us
  blocking collectives: 153 us -> 102 us
  matrix products: 12.4 us -> 31.7 us
  between operations: 0.16 us -> 13.2 us
  local copies, waits for them, and re-layouts: 12.7 us -> 1.8 us
  starting transfers between devices: 7.83 us -> 0.19 us
    reduce_scatter x0 -> x2, waiting for transfers between devices: none -> 195 us  [the longest x1 121 us: shards(): mixture = lax.psum_scatter(mine, 'ep', scatter_dimension=0, tiled=True)]
    all_to_all x3 -> x0, blocking collectives: 150 us -> none  [the longest x1 138 us: shards(): lax.all_to_all(outgoing, 'ep', split_axis=0, concat_axis=0, tiled=True)]
    all_gather x0 -> x2, waiting for transfers between devices: none -> 131 us  [the longest x1 131 us: shards(): part = lax.all_gather(own_half, 'ep', axis=0, tiled=True)]
    all_to_all x1 -> x0, waiting for transfers between devices: 105 us -> none  [shards(): lax.all_to_all(expert_out, 'ep', split_axis=0, concat_axis=0, tiled=True)]
    all_gather x0 -> x2, blocking collectives: none -> 78.7 us  [the longest x1 40.2 us: shards(): all_routes = lax.all_gather(routes, 'ep', axis=0, tiled=True)]
    psum x1, blocking collectives: 2.92 us -> 23.8 us  [shards(): lax.psum((jnp.sum(summed, axis=1), jnp.sum(summed * summed, axis=1)), 'tp')]
    dot_general x3 -> x2, matrix products: 12.4 us -> 31.7 us  [the longest x1 20.3 us: shards(): partial_sum = jnp.dot(hidden, w_down[0], preferred_element_type=jnp.float32)]
    all_to_all x1 -> x0, starting transfers between devices: 7.83 us -> none  [shards(): lax.all_to_all(expert_out, 'ep', split_axis=0, concat_axis=0, tiled=True)]
  transfers between devices with their start and end apart: 1 -> 4, of which waited for: 1 -> 3; matrix products, arithmetic and copies ran while one was open for 0% -> 0% of each run, Pallas kernels for 0% -> 0%
where the time goes in v1:
time: 478 us
  waiting for transfers between devices  326 us (68%)
  blocking collectives  102 us (21%)
  matrix products  31.7 us (7%)
  between operations  13.2 us (3%)
    all_gather x1, waiting for transfers between devices, shards(): part = lax.all_gather(own_half, 'ep', axis=0, tiled=True)  131 us
    reduce_scatter x1, waiting for transfers between devices, shards(): mixture = lax.psum_scatter(mine, 'ep', scatter_dimension=0, tiled=True)  121 us
    reduce_scatter x1, waiting for transfers between devices, shards(): mine = lax.psum_scatter(weighted, 'tp', scatter_dimension=1, tiled=True)  73.7 us
    all_gather x1, blocking collectives, shards(): all_routes = lax.all_gather(routes, 'ep', axis=0, tiled=True)  40.2 us
    all_gather x1, blocking collectives, shards(): all_gates = lax.all_gather(gate_weights, 'ep', axis=0, tiled=True)  38.5 us
    psum x1, blocking collectives, shards(): lax.psum((jnp.sum(summed, axis=1), jnp.sum(summed * summed, axis=1)), 'tp')  23.8 us
    dot_general x1, matrix products, shards(): partial_sum = jnp.dot(hidden, w_down[0], preferred_element_type=jnp.float32)  20.3 us
    dot_general x1, matrix products, shards(): gate = jnp.dot(everyone, w_gate[0], preferred_element_type=jnp.float32)  11.4 us
  transfers between devices with their start and end apart: 4, of which 3 were waited for; matrix products, arithmetic and copies ran while one was open for 0% of the time, Pallas kernels for 0%

profile of v1, /device:TPU:37, one launch (start us, length us, event | category | flops | bytes accessed | tf_op | source)
XLA Modules:
  0.0 478.2 jit_solution(6400377105573818725)
XLA Ops:
  6.5 0.0 copy-start
  6.6 0.0 all-gather.5.cloned.1.call-start
  6.6 1.7 constant_dynamic-slice_fusion
  8.3 0.1 all-gather.5.cloned.1.call-update
  8.3 0.1 all-gather.7.cloned.1.call-start
  8.4 131.1 %all-gather.5.cloned.1.call-done = bf16[2048,1024]{1,0:T(8,128)(2,1)} async-done(((bf16[64,1024]{1,0:T(8,128)(2,1)}), bf16[2048,1024]{1,0:T(8,128)(2,1)}) %all-gather.5.cloned.1.call-update) | async-done | bytes 4194320 | tf_op jit(solution)/shard_map/all_gather | solution.py:17
  139.5 0.1 all-gather.7.cloned.1.call-update
  139.5 0.1 reduce-scatter.3.cloned.1.call-start
  139.6 40.2 %all-gather = s32[32,64,4]{1,2,0:T(4,128)S(1)} all-gather(s32[1,64,4]{1,2,0:T(4,128)} %bitcast.15), channel_id=1, replica_groups=mesh['grp'=4,'ep'=32,'tp'=2] {'ep'}, dimensions={0}, use_global_device_ids=true | all-gather | bytes 33792 | tf_op jit(solution)/shard_map/all_gather | solution.py:19
  179.8 38.5 %all-gather.1 = f32[32,64,4]{1,2,0:T(4,128)S(1)} all-gather(f32[1,64,4]{1,2,0:T(4,128)} %bitcast.16), channel_id=1, replica_groups=mesh['grp'=4,'ep'=32,'tp'=2] {'ep'}, dimensions={0}, use_global_device_ids=true | all-gather | bytes 33792 | tf_op jit(solution)/shard_map/all_gather | solution.py:20
  218.3 0.1 select_reduce_fusion
  218.3 0.1 reshape.15
  218.4 0.0 all-gather.7.cloned.1.call-done
  218.4 11.4 %fusion.4 = f32[2048,640]{1,0:T(8,128)} fusion(bf16[2048,2048]{1,0:T(8,128)(2,1)} %all-gather.7.cloned.1.call-done, bf16[1,2048,640]{2,1,0:T(8,128)(2,1)} %param.11), kind=kOutput, calls=%fused_computation.4 | convolution fusion | flops 5368709120 | bytes 16252928 | tf_op jit(solution)/shard_map/dot_general | solution.py:22
  229.8 0.0 copy-done
  229.8 20.3 %multiply_convert_fusion = bf16[2048,2048]{1,0:T(8,128)(2,1)} fusion(f32[2048]{0:T(1024)S(1)} %reshape.15, bf16[1,640,2048]{2,1,0:T(8,128)(2,1)S(1)} %copy-done, f32[2048,640]{1,0:T(8,128)} %fusion.4, bf16[2048,2048]{1,0:T(8,128)(2,1)} %all-gather.7.cloned.1.call-done, bf16[1,2048,640]{2,1,0:T(8,128)(2,1)} %param.12), kind=kOutput, calls=%fused_computation | convolution fusion | flops 10753671168 | bytes 27271168 | tf_op jit(solution)/shard_map/dot_general | solution.py:25
  250.1 0.0 copy-start.1
  250.1 0.0 copy-start.2
  250.1 0.0 copy-start.3
  250.1 0.1 reduce-scatter.3.cloned.1.call-update
  250.2 0.1 reduce-scatter.5.cloned.1.call-start
  250.3 73.7 %reduce-scatter.3.cloned.1.call-done = bf16[2048,1024]{1,0:T(8,128)(2,1)} async-done(((bf16[2048,2048]{1,0:T(8,128)(2,1)}), bf16[2048,1024]{1,0:T(8,128)(2,1)}) %reduce-scatter.3.cloned.1.call-update) | async-done | bytes 4194320 | tf_op jit(solution)/shard_map/reduce_scatter | solution.py:27
  324.0 0.1 reduce-scatter.5.cloned.1.call-update
  324.1 121.0 %reduce-scatter.5.cloned.1.call-done = bf16[64,1024]{1,0:T(8,128)(2,1)} async-done(((bf16[2048,1024]{1,0:T(8,128)(2,1)}), bf16[64,1024]{1,0:T(8,128)(2,1)}) %reduce-scatter.5.cloned.1.call-update) | async-done | bytes 131088 | tf_op jit(solution)/shard_map/reduce_scatter | solution.py:28
  445.0 0.0 copy-done.1
  445.0 1.1 fusion.7
  446.1 23.8 %all-reduce = (f32[64]{0:T(128)S(1)}, f32[64]{0:T(128)S(1)}) all-reduce(f32[64]{0:T(128)S(1)} %get-tuple-element.6, f32[64]{0:T(128)S(1)} %get-tuple-element.5), channel_id=1, replica_groups=mesh['grp'=4,'ep'=32,'tp'=2] {'tp'}, use_global_device_ids=true, to_apply=%region_6.7 | all-reduce | flops 128 | bytes 1024 | tf_op jit(solution)/shard_map/psum | solution.py:30
  469.9 0.0 copy-done.2
  469.9 0.0 copy-done.3
  469.9 1.7 add_convert_fusion
  (1 shorter events, 0.0 us)
Async XLA Ops:
  6.5 223.2 %copy-start = (bf16[1,640,2048]{2,1,0:T(8,128)(2,1)S(1)}, bf16[1,640,2048]{2,1,0:T(8,128)(2,1)}, u32[]{:S(2)}) copy-start(bf16[1,640,2048]{2,1,0:T(8,128)(2,1)} %param.13) | copy-start | bytes 7864324
  6.6 132.9 %all-gather.5.cloned.1.call-start = ((), (), s32[]{:S(2)}) async-start(), calls=%async_computation.2 | async-start | bytes 4325376 | tf_op jit(solution)/shard_map/all_gather | solution.py:17
  8.3 210.1 %all-gather.7.cloned.1.call-start = ((), (), s32[]{:S(2)}) async-start(), calls=%async_computation.3 | async-start | bytes 12582912 | tf_op jit(solution)/shard_map/all_gather | solution.py:18
  139.5 184.5 %reduce-scatter.3.cloned.1.call-start = ((), (), s32[]{:S(2)}) async-start(), calls=%async_computation.4 | async-start | bytes 12582912 | tf_op jit(solution)/shard_map/reduce_scatter | solution.py:27
  250.1 194.9 %copy-start.1 = (bf16[64,2048]{1,0:T(8,128)(2,1)S(1)}, bf16[64,2048]{1,0:T(8,128)(2,1)}, u32[]{:S(2)}) copy-start(bf16[64,2048]{1,0:T(8,128)(2,1)} %param.8) | copy-start | bytes 786436
  250.1 219.8 %copy-start.2 = (f32[1024]{0:T(1024)S(1)}, f32[1024]{0:T(1024)}, u32[]{:S(2)}) copy-start(f32[1024]{0:T(1024)} %param.15) | copy-start | bytes 12292
  250.1 219.8 %copy-start.3 = (f32[1024]{0:T(1024)S(1)}, f32[1024]{0:T(1024)}, u32[]{:S(2)}) copy-start(f32[1024]{0:T(1024)} %param.14) | copy-start | bytes 12292
  250.2 194.9 %reduce-scatter.5.cloned.1.call-start = ((), (), s32[]{:S(2)}) async-start(), calls=%async_computation.5 | async-start | bytes 4325376 | tf_op jit(solution)/shard_map/reduce_scatter | solution.py:28
Sparse Core Ops, SparseCore 0:
  9.1 130.2 all-gather.4
  141.3 50.2 all-gather.6
  250.3 73.6 reduce-scatter.2
  326.4 118.5 reduce-scatter.4

commit v2 on v1

v2 whole, which is shorter than its diff:
```python
import functools

import jax
import jax.numpy as jnp
from jax import lax
from jax.experimental import pallas as pl
from jax.experimental.pallas import tpu as pltpu
from jax.sharding import PartitionSpec as P

residual_scale = 1.4142135
norm_eps = 1e-05
col_groups = 4
ffn_rows = 128
ffn_cols = 256
bf16, f32 = jnp.bfloat16, jnp.float32


def moe_kernel(
    num_ep, num_experts,
    tokens, meta, w_gate, w_up, w_down, gain, bias, out,
    rows_in, metas, wg, wu, wd, gains, biases, weight_cols, hidden, sums, chain, own_out, other_out,
    disp_recv, disp_send, meta_recv, meta_send, comb_recv, comb_send, local_sems, pair_sems,
):
    me = lax.axis_index("ep")
    core = lax.axis_index("tp")
    other = 1 - core
    half = num_ep // 2
    own_tok = tokens.shape[0] // 2
    width = tokens.shape[1]
    cols = width // col_groups
    part = own_tok // 2
    ff_half = w_down.shape[1]
    ff = 2 * ff_half
    ff_tiles = ff // ffn_cols
    chunks = 2 * col_groups
    slot_rows = 2 * own_tok
    own_row = half * slot_rows - own_tok
    batches = half * slot_rows // ffn_rows
    pairs = half // 2
    first_pair = pairs // 2
    ahead = pairs - first_pair - 1
    last = batches - 1
    targets = ({"ep": lax.rem(me + 1, num_ep)}, {"ep": lax.rem(me + num_ep - 1, num_ep)})
    partner = {"tp": other}

    loads = []
    for g in range(col_groups):
        loads.append(pltpu.make_async_copy(
            tokens.at[pl.ds(core * own_tok, own_tok), pl.ds(g * cols, cols)],
            rows_in.at[g, pl.ds(own_row, own_tok), :],
            local_sems.at[g],
        ))
    own_cols = pl.ds(pl.multiple_of(core * ff_half, 128), ff_half)
    other_cols = pl.ds(pl.multiple_of(other * ff_half, 128), ff_half)
    own_ff = pl.ds(pl.multiple_of(core * ff_half, 128), ff_half)
    other_ff = pl.ds(pl.multiple_of(other * ff_half, 128), ff_half)
    loads.append(pltpu.make_async_copy(meta.at[core], metas.at[num_ep - 1], local_sems.at[col_groups]))
    for load in loads:
        load.start()
    weight_loads = [
        pltpu.make_async_copy(w_gate.at[0], wg.at[:, own_cols], local_sems.at[col_groups + 1]),
        pltpu.make_async_copy(w_up.at[0], wu.at[:, own_cols], local_sems.at[col_groups + 2]),
        pltpu.make_async_copy(w_down.at[0], wd.at[own_ff, :], local_sems.at[col_groups + 3]),
        pltpu.make_async_copy(gain, gains.at[core], local_sems.at[col_groups + 4]),
        pltpu.make_async_copy(bias, biases.at[core], local_sems.at[col_groups + 5]),
    ]

    barrier = pltpu.get_barrier_semaphore()
    for peer in (targets[0], targets[1], partner):
        pl.semaphore_signal(barrier, inc=1, device_id=peer, device_id_type=pl.DeviceIdType.MESH)
    pl.semaphore_wait(barrier, 3)

    for load in loads:
        load.wait()

    def row_half(direction, c):
        first = c // col_groups
        return first if direction == 0 else 1 - first

    def dispatch_copy(direction, step, c):
        r = row_half(direction, c)
        g = lax.rem(c, col_groups)
        src = jnp.where(step == 0, own_row, (step - 1) * slot_rows + direction * own_tok) + r * part
        dst = step * slot_rows + jnp.where(step == half - 1, 0, direction * own_tok) + r * part
        return pltpu.make_async_remote_copy(
            src_ref=rows_in.at[g, pl.ds(pl.multiple_of(src, part), part), :],
            dst_ref=rows_in.at[g, pl.ds(pl.multiple_of(dst, part), part), :],
            send_sem=disp_send.at[direction, lax.rem(step, 2), c],
            recv_sem=disp_recv.at[direction, step, c],
            device_id=targets[direction],
            device_id_type=pl.DeviceIdType.MESH,
        )

    def meta_copy(direction, step):
        src = jnp.where(step == 0, num_ep - 1, (step - 1) * 2 + direction)
        dst = step * 2 + direction
        return pltpu.make_async_remote_copy(
            src_ref=metas.at[src],
            dst_ref=metas.at[dst],
            send_sem=meta_send.at[direction, lax.rem(step, 2)],
            recv_sem=meta_recv.at[direction, step],
            device_id=targets[direction],
            device_id_type=pl.DeviceIdType.MESH,
        )

    for direction in range(2):
        meta_copy(direction, jnp.int32(0)).start()

    @pl.loop(0, chunks)
    def _(c):
        for direction in range(2):
            dispatch_copy(direction, jnp.int32(0), c).start()

    for load in weight_loads:
        load.start()

    def pair_copy(src, dst, k):
        return pltpu.make_async_remote_copy(
            src_ref=src, dst_ref=dst, send_sem=pair_sems.at[0, k], recv_sem=pair_sems.at[1, k],
            device_id=partner, device_id_type=pl.DeviceIdType.MESH,
        )

    gate_steps = first_pair * chunks
    gate_rows = width // gate_steps
    down_rows = 32
    down_steps = ff_half // down_rows
    pair_copy(gain, gains.at[core], 3).start()
    pair_copy(bias, biases.at[core], 4).start()

    def weight_step(kk):
        @pl.when(kk < gate_steps)
        def _():
            rows = pl.ds(pl.multiple_of(kk * gate_rows, gate_rows), gate_rows)
            pair_copy(w_gate.at[0, rows, :], wg.at[rows, own_cols], 0).start()
            pair_copy(w_up.at[0, rows, :], wu.at[rows, own_cols], 1).start()

        @pl.when((kk >= gate_steps) & (kk < gate_steps + down_steps))
        def _():
            at = (kk - gate_steps) * down_rows
            src = pl.ds(pl.multiple_of(at, down_rows), down_rows)
            dst = pl.ds(pl.multiple_of(core * ff_half + at, down_rows), down_rows)
            pair_copy(w_down.at[0, src, :], wd.at[dst, :], 2).start()

    def wait_weights():
        for load in weight_loads:
            load.wait()
        pair_copy(w_gate.at[0], wg.at[:, other_cols], 0).wait_recv()
        pair_copy(w_up.at[0], wu.at[:, other_cols], 1).wait_recv()
        pair_copy(w_down.at[0], wd.at[other_ff, :], 2).wait_recv()
        pair_copy(gain, gains.at[other], 3).wait_recv()
        pair_copy(bias, biases.at[other], 4).wait_recv()

    def weight_column(b):
        per_batch = ffn_rows // own_tok
        lane = lax.broadcasted_iota(jnp.int32, (own_tok, 128), 1)
        sub = lax.broadcasted_iota(jnp.int32, (own_tok, 128), 0)
        mine = lane * own_tok // 128 == sub
        for i in range(per_batch):
            block = metas[b * per_batch + i]
            flat = jnp.where(block[1:2, :] == me.astype(f32), block[0:1, :], 0.0)
            spread = jnp.where(mine, jnp.broadcast_to(flat, (own_tok, 128)), 0.0)
            column = jnp.sum(spread, axis=1, keepdims=True)
            weight_cols[pl.ds(i * own_tok, own_tok), :] = jnp.broadcast_to(column, (own_tok, 128))

    def gate_up(b, j):
        rows = pl.ds(pl.multiple_of(b * ffn_rows, ffn_rows), ffn_rows)
        at = pl.ds(pl.multiple_of(j * ffn_cols, ffn_cols), ffn_cols)
        gate = jnp.zeros((ffn_rows, ffn_cols), f32)
        upper = jnp.zeros((ffn_rows, ffn_cols), f32)
        for g in range(col_groups):
            x = rows_in[g, rows, :]
            gate += jnp.dot(x, wg[pl.ds(g * cols, cols), at], preferred_element_type=f32)
            upper += jnp.dot(x, wu[pl.ds(g * cols, cols), at], preferred_element_type=f32)
        value = gate / (1.0 + jnp.exp(-gate)) * upper * weight_cols[:, 0:1]
        hidden[j] = value.astype(bf16)

    def down(b, g):
        rows = pl.ds(pl.multiple_of(b * ffn_rows, ffn_rows), ffn_rows)
        at = pl.ds(pl.multiple_of(g * cols, cols), cols)
        total = jnp.zeros((ffn_rows, cols), f32)
        for j in range(ff_tiles):
            total += jnp.dot(hidden[j], wd[pl.ds(j * ffn_cols, ffn_cols), at], preferred_element_type=f32)
        sums[g, rows, :] = total

    def ffn_step(b, k):
        @pl.when(k == 0)
        def _():
            weight_column(b)

        @pl.when((lax.rem(k, 2) == 0) & (k < 2 * ff_tiles))
        def _():
            gate_up(b, k // 2)

        @pl.when((k >= 2 * ff_tiles) & (k < 2 * ff_tiles + col_groups))
        def _():
            down(b, k - 2 * ff_tiles)

    @pl.loop(0, half * chunks)
    def _(kk):
        slot = kk // chunks
        c = lax.rem(kk, chunks)
        step = slot + 1

        @pl.when(c == 0)
        def _():
            meta_copy(0, slot).wait_recv()

            @pl.when(step < half)
            def _():
                meta_copy(1, slot).wait_recv()

                @pl.when(step >= 2)
                def _():
                    meta_copy(0, step).wait_send()

                meta_copy(0, step).start()

                @pl.when(step < half - 1)
                def _():
                    @pl.when(step >= 2)
                    def _():
                        meta_copy(1, step).wait_send()

                    meta_copy(1, step).start()

        for direction in range(2):
            @pl.when((step < half) | (c < col_groups))
            def _():
                dispatch_copy(direction, slot, c).wait_recv()

            @pl.when((step < half - 1) | ((step == half - 1) & (c < col_groups)))
            def _():
                @pl.when(step >= 2)
                def _():
                    dispatch_copy(direction, step, c).wait_send()

                dispatch_copy(direction, step, c).start()

        weight_step(kk)
        pair = slot // 2

        @pl.when(kk == first_pair * 2 * chunks)
        def _():
            wait_weights()

        @pl.when(pair >= first_pair)
        def _():
            ffn_step(jnp.where(pair == pairs - 1, last - 1, pair - first_pair), lax.rem(kk, 2 * chunks))

    def chain_rows(age, r):
        return pl.ds(pl.multiple_of(age * own_tok + r * part, part), part)

    def sum_rows(distance, direction, r):
        at = (distance - 1) * slot_rows + jnp.where(distance == half, 0, (1 - direction) * own_tok) + r * part
        return pl.ds(pl.multiple_of(at, part), part)

    def combine_copy(direction, distance, c):
        r = row_half(direction, c)
        g = lax.rem(c, col_groups)
        return pltpu.make_async_remote_copy(
            src_ref=chain.at[direction, g, chain_rows(distance, r), :],
            dst_ref=chain.at[direction, g, chain_rows(distance - 1, r), :],
            send_sem=comb_send.at[direction, lax.rem(distance, 2), c],
            recv_sem=comb_recv.at[direction, distance - 1, c],
            device_id=targets[direction],
            device_id_type=pl.DeviceIdType.MESH,
        )

    weight_column(last)

    @pl.loop(0, ff_tiles)
    def _(j):
        gate_up(last, j)

    @pl.loop(0, col_groups)
    def _(g):
        down(last, g)
        for direction in range(2):
            r = direction
            chain[direction, g, chain_rows(half, r), :] = sums[g, sum_rows(half, direction, r), :].astype(bf16)
            combine_copy(direction, jnp.int32(half), g).start()

    @pl.loop(chunks, half * chunks)
    def _(kk):
        distance = half - kk // chunks
        c = lax.rem(kk, chunks)
        g = lax.rem(c, col_groups)
        for direction in range(2):
            r = row_half(direction, c)
            fresh = (distance == half - 1) & (c >= col_groups)
            mine = sums[g, sum_rows(distance, direction, r), :]

            @pl.when(fresh)
            def _():
                chain[direction, g, chain_rows(distance, r), :] = mine.astype(bf16)

            @pl.when(jnp.logical_not(fresh))
            def _():
                combine_copy(direction, distance + 1, c).wait_recv()
                before = chain[direction, g, chain_rows(distance, r), :].astype(f32)
                chain[direction, g, chain_rows(distance, r), :] = (before + mine).astype(bf16)

            @pl.when((distance <= half - 3) | ((distance == half - 2) & (c < col_groups)))
            def _():
                combine_copy(direction, distance, c).wait_send()

            combine_copy(direction, distance, c).start()

        batch = last - 2 - (kk - chunks) // (2 * chunks)

        @pl.when(batch >= ahead)
        def _():
            ffn_step(batch, lax.rem(kk - chunks, 2 * chunks))

    row_sum = jnp.zeros((own_tok, 1), f32)
    for direction in range(2):
        @pl.loop(0, chunks)
        def _(c):
            combine_copy(direction, jnp.int32(1), c).wait_recv()
    kept = []
    for g in range(col_groups):
        mixture = (
            chain[0, g, 0:own_tok, :].astype(f32)
            + chain[1, g, 0:own_tok, :].astype(f32)
            + sums[g, pl.ds(own_row, own_tok), :]
        ).astype(bf16)
        value = residual_scale * rows_in[g, pl.ds(own_row, own_tok), :].astype(f32) + mixture.astype(f32)
        sums[g, pl.ds(own_row, own_tok), :] = value
        row_sum += jnp.sum(value, axis=1, keepdims=True)
    mean = row_sum / width
    square_sum = jnp.zeros((own_tok, 1), f32)
    for g in range(col_groups):
        value = sums[g, pl.ds(own_row, own_tok), :] - mean
        square_sum += jnp.sum(value * value, axis=1, keepdims=True)
    scale = lax.rsqrt(square_sum / width + norm_eps)
    per_half = col_groups // 2
    for g in range(col_groups):
        at = pl.ds((g % per_half) * cols, cols)
        value = (sums[g, pl.ds(own_row, own_tok), :] - mean) * scale
        own_out[g] = (value * gains[g // per_half, :, at] + biases[g // per_half, :, at]).astype(bf16)
    swap = pair_copy(own_out.at[pl.ds(other * per_half, per_half)], other_out, 5)
    swap.start()
    for g in range(per_half):
        out[pl.ds(core * own_tok, own_tok), pl.ds(g * cols, cols)] = own_out[core * per_half + g]
    swap.wait_recv()
    for g in range(per_half):
        out[pl.ds(other * own_tok, own_tok), pl.ds(g * cols, cols)] = other_out[g]

    swap.wait_send()
    for direction in range(2):
        @pl.loop(0, chunks)
        def _(c):
            for step in (half - 2, half - 1):
                dispatch_copy(direction, jnp.int32(step), c).wait_send()
            for distance in (2, 1):
                combine_copy(direction, jnp.int32(distance), c).wait_send()
        for step in (half - 2, half - 1):
            meta_copy(direction, jnp.int32(step)).wait_send()
    pair_copy(w_gate.at[0], wg.at[:, own_cols], 0).wait_send()
    pair_copy(w_up.at[0], wu.at[:, own_cols], 1).wait_send()
    pair_copy(w_down.at[0], wd.at[own_ff, :], 2).wait_send()
    pair_copy(gain, gains.at[core], 3).wait_send()
    pair_copy(bias, biases.at[core], 4).wait_send()


def shards(tokens, routes, gate_weights, w_gate, w_up, w_down, norm_gain, norm_bias):
    num_ep = lax.axis_size("ep")
    tok_rows, width = tokens.shape
    own_tok = tok_rows // 2
    half = num_ep // 2
    ff = 2 * w_down.shape[1]
    cols = width // col_groups
    chunks = 2 * col_groups
    rows = half * 2 * own_tok
    meta = jnp.stack(
        [gate_weights.reshape(2, own_tok * gate_weights.shape[1]), routes.astype(f32).reshape(2, own_tok * routes.shape[1])],
        axis=1,
    )
    any_spec = pl.BlockSpec(memory_space=pl.ANY)
    dma = pltpu.SemaphoreType.DMA
    return pl.pallas_call(
        functools.partial(moe_kernel, num_ep, num_ep),
        out_shape=jax.ShapeDtypeStruct((tok_rows, width // 2), bf16),
        in_specs=[any_spec] * 7,
        out_specs=pl.BlockSpec(memory_space=pltpu.VMEM),
        scratch_shapes=[
            pltpu.VMEM((col_groups, rows, cols), bf16),
            pltpu.VMEM((num_ep, 2, 128), f32),
            pltpu.VMEM((width, ff), bf16),
            pltpu.VMEM((width, ff), bf16),
            pltpu.VMEM((ff, width), bf16),
            pltpu.VMEM((2, 1, width // 2), f32),
            pltpu.VMEM((2, 1, width // 2), f32),
            pltpu.VMEM((ffn_rows, 128), f32),
            pltpu.VMEM((ff // ffn_cols, ffn_rows, ffn_cols), bf16),
            pltpu.VMEM((col_groups, rows, cols), f32),
            pltpu.VMEM((2, col_groups, (half + 1) * own_tok, cols), bf16),
            pltpu.VMEM((col_groups, own_tok, cols), bf16),
            pltpu.VMEM((col_groups // 2, own_tok, cols), bf16),
            dma((2, half, chunks)),
            dma((2, 2, chunks)),
            dma((2, half)),
            dma((2, 2)),
            dma((2, half, chunks)),
            dma((2, 2, chunks)),
            dma((col_groups + 6,)),
            dma((2, 6)),
        ],
        compiler_params=pltpu.CompilerParams(
            collective_id=0, has_side_effects=True, vmem_limit_bytes=60 * 1024 * 1024
        ),
    )(tokens, meta, w_gate, w_up, w_down, norm_gain.reshape(1, -1), norm_bias.reshape(1, -1))


def solution(mesh):
    in_specs = (
        P(("grp", "ep"), None),
        P(("grp", "ep"), None),
        P(("grp", "ep"), None),
        P("ep", None, "tp"),
        P("ep", None, "tp"),
        P("ep", "tp", None),
        P("tp"),
        P("tp"),
    )
    out_specs = P(("grp", "ep"), "tp")
    return jax.shard_map(shards, mesh=mesh, in_specs=in_specs, out_specs=out_specs, check_vma=False)
```

time: 478 us -> 151 us (0.32)
  waiting for transfers between devices: 326 us -> 0 us
  Pallas kernels: 0 us -> 147 us
  blocking collectives: 102 us -> 0 us
  matrix products: 31.7 us -> 0 us
  between operations: 13.2 us -> 0.02 us
    reduce_scatter x2 -> x0, waiting for transfers between devices: 195 us -> none  [the longest x1 121 us: shards(): mixture = lax.psum_scatter(mine, 'ep', scatter_dimension=0, tiled=True)]
    pallas_call x0 -> x1, Pallas kernels: none -> 147 us  [shards(): pl.pallas_call(functools.partial(moe_kernel, num_ep, num_ep), out_shape=j...]
    all_gather x2 -> x0, waiting for transfers between devices: 131 us -> none  [the longest x1 131 us: shards(): part = lax.all_gather(own_half, 'ep', axis=0, tiled=True)]
    all_gather x2 -> x0, blocking collectives: 78.7 us -> none  [the longest x1 40.2 us: shards(): all_routes = lax.all_gather(routes, 'ep', axis=0, tiled=True)]
    dot_general x2 -> x0, matrix products: 31.7 us -> none  [the longest x1 20.3 us: shards(): partial_sum = jnp.dot(hidden, w_down[0], preferred_element_type=jnp.float32)]
    psum x1 -> x0, blocking collectives: 23.8 us -> none  [shards(): lax.psum((jnp.sum(summed, axis=1), jnp.sum(summed * summed, axis=1)), 'tp')]
  transfers between devices with their start and end apart: 4 -> 0, of which waited for: 3 -> 0; matrix products, arithmetic and copies ran while one was open for 0% -> 0% of each run, Pallas kernels for 0% -> 0%
where the time goes in v2:
time: 151 us
  Pallas kernels  147 us (97%)
  local copies, waits for them, and re-layouts  2.65 us (2%)
    pallas_call x1, Pallas kernels, shards(): pl.pallas_call(functools.partial(moe_kernel, num_ep, num_ep), out_shape=j...  147 us

profile of v2, /device:TPU:37, one launch (start us, length us, event | category | flops | bytes accessed | tf_op | source)
XLA Modules:
  0.0 151.2 jit_solution(13004526703635384061)
XLA Ops:
  0.0 0.7 convert_element_type.3
  0.7 0.1 copy.12
  0.8 0.1 stack_reshape.7
  0.9 0.8 copy.11
  1.7 0.1 stack_reshape.6
  1.8 0.6 pad_maximum_fusion.meta
  2.4 147.3 %shard_map.82 = bf16[64,1024]{1,0:T(8,128)(2,1)} custom-call(bf16[64,2048]{1,0:T(8,128)(2,1)} %tokens.1, f32[2,2,128]{2,1,0:T(2,128)} %pad_maximum_fusion.meta, bf16[1,2048,640]{2,1,0:T(8,128)(2,1)} %w_gate.1, bf16[1,2048,640]{2,1,0:T(8,128)(2,1)} %w_up.1, bf16[1,640,2048]{2,1,0:T(8,128)(2,1)} %w_down.1, f32[1,1024]{1,0:T(1,128)} %bitcast.4, f32[1,1024]{1,0:T(1,128)} %bitcast.5), custom_call_target="tpu_custom_call" | custom-call | tf_op jit(solution)/shard_map/pallas_call | solution.py:381
  149.6 1.6 %copy.16 = bf16[64,1024]{1,0:T(8,128)(2,1)} copy(bf16[64,1024]{1,0:T(8,128)(2,1)} %shard_map.82) | data formatting | bytes 262144

commit v3 on v1

v3 whole, which is shorter than its diff:
```python
import functools

import jax
import jax.numpy as jnp
from jax import lax
from jax.experimental import pallas as pl
from jax.experimental.pallas import tpu as pltpu
from jax.sharding import PartitionSpec as P

residual_scale = 1.4142135
norm_eps = 1e-05
col_groups = 4
ffn_cols = 256
down_steps = 2
bf16, f32 = jnp.bfloat16, jnp.float32


def hops_of(num_ep):
    longer = 2 * ((9 * num_ep) // 32)
    return longer, num_ep - 1 - longer


def moe_kernel(
    num_ep,
    tokens, meta, w_gate, w_up, w_down, gain, bias, out,
    rows_in, metas, wg, wu, wd, gains, biases, weight_cols, hidden, sums, chain, swap_in, own_out, other_out,
    disp_recv, disp_send, meta_recv, meta_send, comb_recv, comb_send, swap_sems, local_sems, pair_sems,
):
    me = lax.axis_index("ep")
    core = lax.axis_index("tp")
    other = 1 - core
    longer, shorter = hops_of(num_ep)
    hops = jnp.where(core == 1, longer, shorter)
    tok, width = tokens.shape
    half_tok = tok // 2
    cols = width // col_groups
    ff_half = w_down.shape[1]
    ff = 2 * ff_half
    ff_tiles = ff // ffn_cols
    chunks = col_groups
    shift = jnp.where(core == 1, 1, 0)
    own_slot = jnp.where(core == 1, longer, 0)
    batches = (hops + 1) // 2
    first_pair = batches // 2
    last = batches - 1
    up, under = lax.rem(me + 1, num_ep), lax.rem(me + num_ep - 1, num_ep)
    disp_target = {"ep": jnp.where(core == 1, up, under)}
    comb_target = {"ep": jnp.where(core == 1, under, up)}
    partner = {"tp": other}
    mesh_ids = pl.DeviceIdType.MESH

    def slot_rows(slot):
        return pl.ds(pl.multiple_of(slot * tok, tok), tok)

    loads = [
        pltpu.make_async_copy(tokens.at[:, pl.ds(g * cols, cols)], rows_in.at[g, slot_rows(own_slot), :], local_sems.at[g])
        for g in range(col_groups)
    ]
    loads.append(pltpu.make_async_copy(meta, metas.at[own_slot], local_sems.at[col_groups]))
    for load in loads:
        load.start()
    own_cols = pl.ds(pl.multiple_of(core * ff_half, 128), ff_half)
    other_cols = pl.ds(pl.multiple_of(other * ff_half, 128), ff_half)
    weight_loads = [
        pltpu.make_async_copy(w_gate.at[0], wg.at[:, own_cols], local_sems.at[col_groups + 1]),
        pltpu.make_async_copy(w_up.at[0], wu.at[:, own_cols], local_sems.at[col_groups + 2]),
        pltpu.make_async_copy(w_down.at[0], wd.at[own_cols, :], local_sems.at[col_groups + 3]),
        pltpu.make_async_copy(gain, gains.at[core], local_sems.at[col_groups + 4]),
        pltpu.make_async_copy(bias, biases.at[core], local_sems.at[col_groups + 5]),
    ]

    barrier = pltpu.get_barrier_semaphore()
    for peer in ({"ep": up}, {"ep": under}, partner):
        pl.semaphore_signal(barrier, inc=1, device_id=peer, device_id_type=mesh_ids)
    pl.semaphore_wait(barrier, 3)

    for load in loads:
        load.wait()

    def slot_of(age):
        return jnp.where(age == 0, own_slot, age - shift)

    def dispatch_copy(age, c):
        return pltpu.make_async_remote_copy(
            src_ref=rows_in.at[c, slot_rows(slot_of(age)), :],
            dst_ref=rows_in.at[c, slot_rows(age + 1 - shift), :],
            send_sem=disp_send.at[lax.rem(age, 2), c],
            recv_sem=disp_recv.at[age, c],
            device_id=disp_target,
            device_id_type=mesh_ids,
        )

    def meta_copy(age):
        return pltpu.make_async_remote_copy(
            src_ref=metas.at[slot_of(age)],
            dst_ref=metas.at[age + 1 - shift],
            send_sem=meta_send.at[lax.rem(age, 2)],
            recv_sem=meta_recv.at[age],
            device_id=disp_target,
            device_id_type=mesh_ids,
        )

    def combine_copy(distance, c):
        return pltpu.make_async_remote_copy(
            src_ref=chain.at[c, slot_rows(distance), :],
            dst_ref=chain.at[c, slot_rows(distance - 1), :],
            send_sem=comb_send.at[lax.rem(distance, 2), c],
            recv_sem=comb_recv.at[distance - 1, c],
            device_id=comb_target,
            device_id_type=mesh_ids,
        )

    def pair_copy(src, dst, k):
        return pltpu.make_async_remote_copy(
            src_ref=src, dst_ref=dst, send_sem=pair_sems.at[0, k], recv_sem=pair_sems.at[1, k],
            device_id=partner, device_id_type=mesh_ids,
        )

    meta_copy(jnp.int32(0)).start()
    for c in range(chunks):
        dispatch_copy(jnp.int32(0), c).start()
    for load in weight_loads:
        load.start()
    pair_copy(gain, gains.at[core], 3).start()
    pair_copy(bias, biases.at[core], 4).start()

    free_steps = chunks * (2 * (((shorter + 1) // 2) // 2) - 1)
    gate_steps = 1 << (free_steps.bit_length() - 1)
    gate_rows = width // gate_steps
    down_rows = ff_half // free_steps

    def weight_step(kk):
        @pl.when(kk < gate_steps)
        def _():
            rows = pl.ds(pl.multiple_of(kk * gate_rows, gate_rows), gate_rows)
            pair_copy(w_gate.at[0, rows, :], wg.at[rows, own_cols], 0).start()
            pair_copy(w_up.at[0, rows, :], wu.at[rows, own_cols], 1).start()

        @pl.when(kk < free_steps)
        def _():
            src = pl.ds(pl.multiple_of(kk * down_rows, down_rows), down_rows)
            dst = pl.ds(pl.multiple_of(core * ff_half + kk * down_rows, down_rows), down_rows)
            pair_copy(w_down.at[0, src, :], wd.at[dst, :], 2).start()

    def wait_weights():
        for load in weight_loads:
            load.wait()
        pair_copy(w_gate.at[0], wg.at[:, other_cols], 0).wait_recv()
        pair_copy(w_up.at[0], wu.at[:, other_cols], 1).wait_recv()
        pair_copy(w_down.at[0], wd.at[other_cols, :], 2).wait_recv()
        pair_copy(gain, gains.at[other], 3).wait_recv()
        pair_copy(bias, biases.at[other], 4).wait_recv()

    def weight_column(b):
        pairs_per_block = meta.shape[1]
        lane = lax.broadcasted_iota(jnp.int32, (tok, pairs_per_block), 1)
        sub = lax.broadcasted_iota(jnp.int32, (tok, pairs_per_block), 0)
        mine = lane * tok // pairs_per_block == sub
        for i in range(2):
            block = metas[b * 2 + i]
            flat = jnp.where(block[1:2, :] == me.astype(f32), block[0:1, :], 0.0)
            spread = jnp.where(mine, jnp.broadcast_to(flat, (tok, pairs_per_block)), 0.0)
            column = jnp.sum(spread, axis=1, keepdims=True)
            weight_cols[pl.ds(i * tok, tok), :] = jnp.broadcast_to(column, (tok, 128))

    def batch_rows(b):
        return pl.ds(pl.multiple_of(b * 2 * tok, 2 * tok), 2 * tok)

    def gate_up(b, j):
        at = pl.ds(pl.multiple_of(j * ffn_cols, ffn_cols), ffn_cols)
        gate = jnp.zeros((2 * tok, ffn_cols), f32)
        upper = jnp.zeros((2 * tok, ffn_cols), f32)
        for g in range(col_groups):
            x = rows_in[g, batch_rows(b), :]
            gate += jnp.dot(x, wg[pl.ds(g * cols, cols), at], preferred_element_type=f32)
            upper += jnp.dot(x, wu[pl.ds(g * cols, cols), at], preferred_element_type=f32)
        value = gate / (1.0 + jnp.exp(-gate)) * upper * weight_cols[:, 0:1]
        hidden[j] = value.astype(bf16)

    def down(b, g):
        at = pl.ds(pl.multiple_of(g * cols, cols), cols)
        total = jnp.zeros((2 * tok, cols), f32)
        for j in range(ff_tiles):
            total += jnp.dot(hidden[j], wd[pl.ds(j * ffn_cols, ffn_cols), at], preferred_element_type=f32)
        sums[g, batch_rows(b), :] = total

    def ffn_step(b, k):
        @pl.when(k == 0)
        def _():
            weight_column(b)

        @pl.when(k < ff_tiles)
        def _():
            gate_up(b, k)

        @pl.when((k >= ff_tiles) & (k < ff_tiles + down_steps))
        def _():
            for i in range(col_groups // down_steps):
                down(b, (k - ff_tiles) * (col_groups // down_steps) + i)

    @pl.loop(0, hops * chunks)
    def _(kk):
        age = kk // chunks
        c = lax.rem(kk, chunks)
        forward = age + 1 < hops

        @pl.when(c == 0)
        def _():
            meta_copy(age).wait_recv()

            @pl.when(forward)
            def _():
                @pl.when(age >= 1)
                def _():
                    meta_copy(age + 1).wait_send()

                meta_copy(age + 1).start()

        dispatch_copy(age, c).wait_recv()

        @pl.when(forward)
        def _():
            @pl.when(age >= 1)
            def _():
                dispatch_copy(age + 1, c).wait_send()

            dispatch_copy(age + 1, c).start()

        weight_step(kk)
        slot = age + 1 - shift
        pair = slot // 2
        k = lax.rem(slot, 2) * chunks + c

        @pl.when((pair == first_pair) & (k == 0))
        def _():
            wait_weights()

        @pl.when(pair >= first_pair)
        def _():
            ffn_step(jnp.where(pair == last, last - 1, pair - first_pair), k)

    weight_column(last)

    @pl.loop(0, ff_tiles)
    def _(j):
        gate_up(last, j)

    @pl.loop(0, chunks)
    def _(g):
        down(last, g)
        chain[g, slot_rows(hops), :] = sums[g, slot_rows(hops - shift), :].astype(bf16)
        combine_copy(hops, g).start()

    @pl.loop(0, (hops - 1) * chunks)
    def _(kk):
        distance = hops - 1 - kk // chunks
        c = lax.rem(kk, chunks)
        combine_copy(distance + 1, c).wait_recv()
        before = chain[c, slot_rows(distance), :].astype(f32)
        chain[c, slot_rows(distance), :] = (before + sums[c, slot_rows(distance - shift), :]).astype(bf16)

        @pl.when(distance <= hops - 2)
        def _():
            combine_copy(distance, c).wait_send()

        combine_copy(distance, c).start()
        pair = kk // (2 * chunks)
        batch = last - 2 - pair

        @pl.when(batch >= last - first_pair)
        def _():
            ffn_step(batch, lax.rem(kk, 2 * chunks))

    own_half = pl.ds(pl.multiple_of(core * half_tok, half_tok), half_tok)
    other_half = pl.ds(pl.multiple_of(other * half_tok, half_tok), half_tok)

    def swap_copy(g):
        return pltpu.make_async_remote_copy(
            src_ref=chain.at[g, other_half, :], dst_ref=swap_in.at[g],
            send_sem=swap_sems.at[0, g], recv_sem=swap_sems.at[1, g],
            device_id=partner, device_id_type=mesh_ids,
        )

    for g in range(col_groups):
        combine_copy(jnp.int32(1), g).wait_recv()

        @pl.when(core == 0)
        def _():
            chain[g, 0:tok, :] = (chain[g, 0:tok, :].astype(f32) + sums[g, 0:tok, :]).astype(bf16)

        swap_copy(g).start()
    own_rows = pl.ds(pl.multiple_of(own_slot * tok + core * half_tok, half_tok), half_tok)
    row_sum = jnp.zeros((half_tok, 1), f32)
    for g in range(col_groups):
        swap_copy(g).wait_recv()
        mixture = (chain[g, own_half, :].astype(f32) + swap_in[g].astype(f32)).astype(bf16)
        value = residual_scale * rows_in[g, own_rows, :].astype(f32) + mixture.astype(f32)
        sums[g, own_half, :] = value
        row_sum += jnp.sum(value, axis=1, keepdims=True)
    mean = row_sum / width
    square_sum = jnp.zeros((half_tok, 1), f32)
    for g in range(col_groups):
        value = sums[g, own_half, :] - mean
        square_sum += jnp.sum(value * value, axis=1, keepdims=True)
    scale = lax.rsqrt(square_sum / width + norm_eps)
    per_half = col_groups // 2
    for g in range(col_groups):
        at = pl.ds((g % per_half) * cols, cols)
        value = (sums[g, own_half, :] - mean) * scale
        own_out[g] = (value * gains[g // per_half, :, at] + biases[g // per_half, :, at]).astype(bf16)
    trade = pair_copy(own_out.at[pl.ds(other * per_half, per_half)], other_out, 5)
    trade.start()
    for g in range(per_half):
        out[own_half, pl.ds(g * cols, cols)] = own_out[core * per_half + g]
    trade.wait_recv()
    for g in range(per_half):
        out[other_half, pl.ds(g * cols, cols)] = other_out[g]

    trade.wait_send()
    for c in range(chunks):
        swap_copy(c).wait_send()
        for back in (2, 1):
            dispatch_copy(hops - back, c).wait_send()
            combine_copy(jnp.int32(back), c).wait_send()
    for back in (2, 1):
        meta_copy(hops - back).wait_send()
    pair_copy(w_gate.at[0], wg.at[:, own_cols], 0).wait_send()
    pair_copy(w_up.at[0], wu.at[:, own_cols], 1).wait_send()
    pair_copy(w_down.at[0], wd.at[own_cols, :], 2).wait_send()
    pair_copy(gain, gains.at[core], 3).wait_send()
    pair_copy(bias, biases.at[core], 4).wait_send()


def shards(tokens, routes, gate_weights, w_gate, w_up, w_down, norm_gain, norm_bias):
    num_ep = lax.axis_size("ep")
    tok, width = tokens.shape
    ff = 2 * w_down.shape[1]
    cols = width // col_groups
    slots = hops_of(num_ep)[0] + 1
    pairs_per_block = routes.size
    meta = jnp.stack([gate_weights.reshape(pairs_per_block), routes.astype(f32).reshape(pairs_per_block)])
    any_spec = pl.BlockSpec(memory_space=pl.ANY)
    dma = pltpu.SemaphoreType.DMA
    return pl.pallas_call(
        functools.partial(moe_kernel, num_ep),
        out_shape=jax.ShapeDtypeStruct((tok, width // 2), bf16),
        in_specs=[any_spec] * 7,
        out_specs=pl.BlockSpec(memory_space=pltpu.VMEM),
        scratch_shapes=[
            pltpu.VMEM((col_groups, slots * tok, cols), bf16),
            pltpu.VMEM((slots, 2, pairs_per_block), f32),
            pltpu.VMEM((width, ff), bf16),
            pltpu.VMEM((width, ff), bf16),
            pltpu.VMEM((ff, width), bf16),
            pltpu.VMEM((2, 1, width // 2), f32),
            pltpu.VMEM((2, 1, width // 2), f32),
            pltpu.VMEM((2 * tok, 128), f32),
            pltpu.VMEM((ff // ffn_cols, 2 * tok, ffn_cols), bf16),
            pltpu.VMEM((col_groups, slots * tok, cols), f32),
            pltpu.VMEM((col_groups, slots * tok, cols), bf16),
            pltpu.VMEM((col_groups, tok // 2, cols), bf16),
            pltpu.VMEM((col_groups, tok // 2, cols), bf16),
            pltpu.VMEM((col_groups // 2, tok // 2, cols), bf16),
            dma((slots, col_groups)),
            dma((2, col_groups)),
            dma((slots,)),
            dma((2,)),
            dma((slots, col_groups)),
            dma((2, col_groups)),
            dma((2, col_groups)),
            dma((col_groups + 6,)),
            dma((2, 6)),
        ],
        compiler_params=pltpu.CompilerParams(
            collective_id=0, has_side_effects=True, vmem_limit_bytes=60 * 1024 * 1024
        ),
    )(tokens, meta, w_gate, w_up, w_down, norm_gain.reshape(1, -1), norm_bias.reshape(1, -1))


def solution(mesh):
    in_specs = (
        P(("grp", "ep"), None),
        P(("grp", "ep"), None),
        P(("grp", "ep"), None),
        P("ep", None, "tp"),
        P("ep", None, "tp"),
        P("ep", "tp", None),
        P("tp"),
        P("tp"),
    )
    out_specs = P(("grp", "ep"), "tp")
    return jax.shard_map(shards, mesh=mesh, in_specs=in_specs, out_specs=out_specs, check_vma=False)
```

time: 478 us -> 146 us (0.31)
  waiting for transfers between devices: 326 us -> 0 us
  Pallas kernels: 0 us -> 142 us
  blocking collectives: 102 us -> 0 us
  matrix products: 31.7 us -> 0 us
  between operations: 13.2 us -> 0.02 us
    reduce_scatter x2 -> x0, waiting for transfers between devices: 195 us -> none  [the longest x1 121 us: shards(): mixture = lax.psum_scatter(mine, 'ep', scatter_dimension=0, tiled=True)]
    pallas_call x0 -> x1, Pallas kernels: none -> 142 us  [shards(): pl.pallas_call(functools.partial(moe_kernel, num_ep), out_shape=jax.Shape...]
    all_gather x2 -> x0, waiting for transfers between devices: 131 us -> none  [the longest x1 131 us: shards(): part = lax.all_gather(own_half, 'ep', axis=0, tiled=True)]
    all_gather x2 -> x0, blocking collectives: 78.7 us -> none  [the longest x1 40.2 us: shards(): all_routes = lax.all_gather(routes, 'ep', axis=0, tiled=True)]
    dot_general x2 -> x0, matrix products: 31.7 us -> none  [the longest x1 20.3 us: shards(): partial_sum = jnp.dot(hidden, w_down[0], preferred_element_type=jnp.float32)]
    psum x1 -> x0, blocking collectives: 23.8 us -> none  [shards(): lax.psum((jnp.sum(summed, axis=1), jnp.sum(summed * summed, axis=1)), 'tp')]
  transfers between devices with their start and end apart: 4 -> 0, of which waited for: 3 -> 0; matrix products, arithmetic and copies ran while one was open for 0% -> 0% of each run, Pallas kernels for 0% -> 0%
where the time goes in v3:
time: 146 us
  Pallas kernels  142 us (97%)
  local copies, waits for them, and re-layouts  2.65 us (2%)
    pallas_call x1, Pallas kernels, shards(): pl.pallas_call(functools.partial(moe_kernel, num_ep), out_shape=jax.Shape...  142 us

profile of v3, /device:TPU:37, one launch (start us, length us, event | category | flops | bytes accessed | tf_op | source)
XLA Modules:
  0.0 145.9 jit_solution(10758968425579925771)
XLA Ops:
  0.0 0.7 convert_element_type.3
  0.7 0.1 copy.12
  0.8 0.1 stack_reshape.7
  0.9 0.8 copy.11
  1.7 0.1 stack_reshape.6
  1.8 0.6 pad_maximum_fusion.meta
  2.4 141.9 %shard_map.82 = bf16[64,1024]{1,0:T(8,128)(2,1)} custom-call(bf16[64,2048]{1,0:T(8,128)(2,1)} %tokens.1, f32[2,256]{1,0:T(2,128)} %pad_maximum_fusion.meta, bf16[1,2048,640]{2,1,0:T(8,128)(2,1)} %w_gate.1, bf16[1,2048,640]{2,1,0:T(8,128)(2,1)} %w_up.1, bf16[1,640,2048]{2,1,0:T(8,128)(2,1)} %w_down.1, f32[1,1024]{1,0:T(1,128)} %bitcast.2, f32[1,1024]{1,0:T(1,128)} %bitcast.3), custom_call_target="tpu_custom_call" | custom-call | tf_op jit(solution)/shard_map/pallas_call | solution.py:344
  144.3 1.6 %copy.14 = bf16[64,1024]{1,0:T(8,128)(2,1)} copy(bf16[64,1024]{1,0:T(8,128)(2,1)} %shard_map.82) | data formatting | bytes 262144

commit v4 on v3

--- a/solution.py
+++ b/solution.py
@@ -16,14 +16,14 @@
 
 
 def hops_of(num_ep):
-    longer = 2 * ((9 * num_ep) // 32)
+    longer = (17 * num_ep // 32) | 1
     return longer, num_ep - 1 - longer
 
 
 def moe_kernel(
     num_ep,
-    tokens, meta, w_gate, w_up, w_down, gain, bias, out,
-    rows_in, metas, wg, wu, wd, gains, biases, weight_cols, hidden, sums, chain, swap_in, own_out, other_out,
+    tokens, routes, gate_weights, w_gate, w_up, w_down, out,
+    rows_in, routes_in, gates_in, metas, wg, wu, wd, weight_cols, hidden, sums, chain, swap_in, own_out,
     disp_recv, disp_send, meta_recv, meta_send, comb_recv, comb_send, swap_sems, local_sems, pair_sems,
 ):
     me = lax.axis_index("ep")
@@ -33,13 +33,14 @@
     hops = jnp.where(core == 1, longer, shorter)
     tok, width = tokens.shape
     half_tok = tok // 2
+    top = routes.shape[0]
     cols = width // col_groups
     ff_half = w_down.shape[1]
     ff = 2 * ff_half
     ff_tiles = ff // ffn_cols
     chunks = col_groups
-    shift = jnp.where(core == 1, 1, 0)
-    own_slot = jnp.where(core == 1, longer, 0)
+    shift = jnp.where(core == 1, 0, 1)
+    own_slot = jnp.where(core == 1, 0, shorter)
     batches = (hops + 1) // 2
     first_pair = batches // 2
     last = batches - 1
@@ -56,7 +57,8 @@
         pltpu.make_async_copy(tokens.at[:, pl.ds(g * cols, cols)], rows_in.at[g, slot_rows(own_slot), :], local_sems.at[g])
         for g in range(col_groups)
     ]
-    loads.append(pltpu.make_async_copy(meta, metas.at[own_slot], local_sems.at[col_groups]))
+    loads.append(pltpu.make_async_copy(routes, routes_in, local_sems.at[col_groups]))
+    loads.append(pltpu.make_async_copy(gate_weights, gates_in, local_sems.at[col_groups + 4]))
     for load in loads:
         load.start()
     own_cols = pl.ds(pl.multiple_of(core * ff_half, 128), ff_half)
@@ -65,17 +67,19 @@
         pltpu.make_async_copy(w_gate.at[0], wg.at[:, own_cols], local_sems.at[col_groups + 1]),
         pltpu.make_async_copy(w_up.at[0], wu.at[:, own_cols], local_sems.at[col_groups + 2]),
         pltpu.make_async_copy(w_down.at[0], wd.at[own_cols, :], local_sems.at[col_groups + 3]),
-        pltpu.make_async_copy(gain, gains.at[core], local_sems.at[col_groups + 4]),
-        pltpu.make_async_copy(bias, biases.at[core], local_sems.at[col_groups + 5]),
     ]
 
     barrier = pltpu.get_barrier_semaphore()
     for peer in ({"ep": up}, {"ep": under}, partner):
         pl.semaphore_signal(barrier, inc=1, device_id=peer, device_id_type=mesh_ids)
-    pl.semaphore_wait(barrier, 3)
 
     for load in loads:
         load.wait()
+    lane = lax.broadcasted_iota(jnp.int32, (tok, tok), 1)
+    sub = lax.broadcasted_iota(jnp.int32, (tok, tok), 0)
+    metas[own_slot, 0:top, :] = routes_in[...].astype(f32)
+    metas[own_slot, top:2 * top, :] = gates_in[...]
+    pl.semaphore_wait(barrier, 3)
 
     def slot_of(age):
         return jnp.where(age == 0, own_slot, age - shift)
@@ -116,15 +120,13 @@
             device_id=partner, device_id_type=mesh_ids,
         )
 
-    meta_copy(jnp.int32(0)).start()
     for c in range(chunks):
         dispatch_copy(jnp.int32(0), c).start()
+    meta_copy(jnp.int32(0)).start()
     for load in weight_loads:
         load.start()
-    pair_copy(gain, gains.at[core], 3).start()
-    pair_copy(bias, biases.at[core], 4).start()
-
-    free_steps = chunks * (2 * (((shorter + 1) // 2) // 2) - 1)
+
+    free_steps = min(chunks * 2 * (shorter // 4), ff_half // 32)
     gate_steps = 1 << (free_steps.bit_length() - 1)
     gate_rows = width // gate_steps
     down_rows = ff_half // free_steps
@@ -148,18 +150,14 @@
         pair_copy(w_gate.at[0], wg.at[:, other_cols], 0).wait_recv()
         pair_copy(w_up.at[0], wu.at[:, other_cols], 1).wait_recv()
         pair_copy(w_down.at[0], wd.at[other_cols, :], 2).wait_recv()
-        pair_copy(gain, gains.at[other], 3).wait_recv()
-        pair_copy(bias, biases.at[other], 4).wait_recv()
 
     def weight_column(b):
-        pairs_per_block = meta.shape[1]
-        lane = lax.broadcasted_iota(jnp.int32, (tok, pairs_per_block), 1)
-        sub = lax.broadcasted_iota(jnp.int32, (tok, pairs_per_block), 0)
-        mine = lane * tok // pairs_per_block == sub
         for i in range(2):
             block = metas[b * 2 + i]
-            flat = jnp.where(block[1:2, :] == me.astype(f32), block[0:1, :], 0.0)
-            spread = jnp.where(mine, jnp.broadcast_to(flat, (tok, pairs_per_block)), 0.0)
+            row = jnp.zeros((1, tok), f32)
+            for k in range(top):
+                row += jnp.where(block[k:k + 1, :] == me.astype(f32), block[top + k:top + k + 1, :], 0.0)
+            spread = jnp.where(lane == sub, jnp.broadcast_to(row, (tok, tok)), 0.0)
             column = jnp.sum(spread, axis=1, keepdims=True)
             weight_cols[pl.ds(i * tok, tok), :] = jnp.broadcast_to(column, (tok, 128))
 
@@ -204,7 +202,17 @@
         c = lax.rem(kk, chunks)
         forward = age + 1 < hops
 
-        @pl.when(c == 0)
+        @pl.when(forward & (age >= 1))
+        def _():
+            dispatch_copy(age + 1, c).wait_send()
+
+        dispatch_copy(age, c).wait_recv()
+
+        @pl.when(forward)
+        def _():
+            dispatch_copy(age + 1, c).start()
+
+        @pl.when(c == chunks - 1)
         def _():
             meta_copy(age).wait_recv()
 
@@ -216,16 +224,6 @@
 
                 meta_copy(age + 1).start()
 
-        dispatch_copy(age, c).wait_recv()
-
-        @pl.when(forward)
-        def _():
-            @pl.when(age >= 1)
-            def _():
-                dispatch_copy(age + 1, c).wait_send()
-
-            dispatch_copy(age + 1, c).start()
-
         weight_step(kk)
         slot = age + 1 - shift
         pair = slot // 2
@@ -255,14 +253,14 @@
     def _(kk):
         distance = hops - 1 - kk // chunks
         c = lax.rem(kk, chunks)
+        @pl.when(distance <= hops - 2)
+        def _():
+            combine_copy(distance, c).wait_send()
+
         combine_copy(distance + 1, c).wait_recv()
         before = chain[c, slot_rows(distance), :].astype(f32)
         chain[c, slot_rows(distance), :] = (before + sums[c, slot_rows(distance - shift), :]).astype(bf16)
 
-        @pl.when(distance <= hops - 2)
-        def _():
-            combine_copy(distance, c).wait_send()
-
         combine_copy(distance, c).start()
         pair = kk // (2 * chunks)
         batch = last - 2 - pair
@@ -284,7 +282,7 @@
     for g in range(col_groups):
         combine_copy(jnp.int32(1), g).wait_recv()
 
-        @pl.when(core == 0)
+        @pl.when(core == 1)
         def _():
             chain[g, 0:tok, :] = (chain[g, 0:tok, :].astype(f32) + sums[g, 0:tok, :]).astype(bf16)
 
@@ -305,18 +303,24 @@
     scale = lax.rsqrt(square_sum / width + norm_eps)
     per_half = col_groups // 2
     for g in range(col_groups):
-        at = pl.ds((g % per_half) * cols, cols)
-        value = (sums[g, own_half, :] - mean) * scale
-        own_out[g] = (value * gains[g // per_half, :, at] + biases[g // per_half, :, at]).astype(bf16)
-    trade = pair_copy(own_out.at[pl.ds(other * per_half, per_half)], other_out, 5)
-    trade.start()
+        own_out[g] = (sums[g, own_half, :] - mean) * scale
+    trades = [
+        pltpu.make_async_remote_copy(
+            src_ref=own_out.at[other * per_half + g], dst_ref=out.at[own_half, pl.ds(g * cols, cols)],
+            send_sem=pair_sems.at[0, 3 + g], recv_sem=pair_sems.at[1, 3 + g],
+            device_id=partner, device_id_type=mesh_ids,
+        )
+        for g in range(per_half)
+    ]
+    for trade in trades:
+        trade.start()
     for g in range(per_half):
         out[own_half, pl.ds(g * cols, cols)] = own_out[core * per_half + g]
-    trade.wait_recv()
-    for g in range(per_half):
-        out[other_half, pl.ds(g * cols, cols)] = other_out[g]
-
-    trade.wait_send()
+    for trade in trades:
+        trade.wait_recv()
+
+    for trade in trades:
+        trade.wait_send()
     for c in range(chunks):
         swap_copy(c).wait_send()
         for back in (2, 1):
@@ -327,8 +331,6 @@
     pair_copy(w_gate.at[0], wg.at[:, own_cols], 0).wait_send()
     pair_copy(w_up.at[0], wu.at[:, own_cols], 1).wait_send()
     pair_copy(w_down.at[0], wd.at[own_cols, :], 2).wait_send()
-    pair_copy(gain, gains.at[core], 3).wait_send()
-    pair_copy(bias, biases.at[core], 4).wait_send()
 
 
 def shards(tokens, routes, gate_weights, w_gate, w_up, w_down, norm_gain, norm_bias):
@@ -337,30 +339,27 @@
     ff = 2 * w_down.shape[1]
     cols = width // col_groups
     slots = hops_of(num_ep)[0] + 1
-    pairs_per_block = routes.size
-    meta = jnp.stack([gate_weights.reshape(pairs_per_block), routes.astype(f32).reshape(pairs_per_block)])
     any_spec = pl.BlockSpec(memory_space=pl.ANY)
     dma = pltpu.SemaphoreType.DMA
-    return pl.pallas_call(
+    rows = pl.pallas_call(
         functools.partial(moe_kernel, num_ep),
-        out_shape=jax.ShapeDtypeStruct((tok, width // 2), bf16),
-        in_specs=[any_spec] * 7,
+        out_shape=jax.ShapeDtypeStruct((tok, width // 2), f32),
+        in_specs=[any_spec] * 6,
         out_specs=pl.BlockSpec(memory_space=pltpu.VMEM),
         scratch_shapes=[
             pltpu.VMEM((col_groups, slots * tok, cols), bf16),
-            pltpu.VMEM((slots, 2, pairs_per_block), f32),
+            pltpu.VMEM(routes.shape[::-1], jnp.int32),
+            pltpu.VMEM(routes.shape[::-1], f32),
+            pltpu.VMEM((slots, 2 * routes.shape[1], tok), f32),
             pltpu.VMEM((width, ff), bf16),
             pltpu.VMEM((width, ff), bf16),
             pltpu.VMEM((ff, width), bf16),
-            pltpu.VMEM((2, 1, width // 2), f32),
-            pltpu.VMEM((2, 1, width // 2), f32),
             pltpu.VMEM((2 * tok, 128), f32),
             pltpu.VMEM((ff // ffn_cols, 2 * tok, ffn_cols), bf16),
             pltpu.VMEM((col_groups, slots * tok, cols), f32),
             pltpu.VMEM((col_groups, slots * tok, cols), bf16),
             pltpu.VMEM((col_groups, tok // 2, cols), bf16),
-            pltpu.VMEM((col_groups, tok // 2, cols), bf16),
-            pltpu.VMEM((col_groups // 2, tok // 2, cols), bf16),
+            pltpu.VMEM((col_groups, tok // 2, cols), f32),
             dma((slots, col_groups)),
             dma((2, col_groups)),
             dma((slots,)),
@@ -374,7 +373,8 @@
         compiler_params=pltpu.CompilerParams(
             collective_id=0, has_side_effects=True, vmem_limit_bytes=60 * 1024 * 1024
         ),
-    )(tokens, meta, w_gate, w_up, w_down, norm_gain.reshape(1, -1), norm_bias.reshape(1, -1))
+    )(tokens, routes.T, gate_weights.T, w_gate, w_up, w_down)
+    return (rows * norm_gain + norm_bias).astype(bf16)
 
 
 def solution(mesh):

time: 146 us -> 134 us (0.918)
  Pallas kernels: 142 us -> 132 us
  local copies, waits for them, and re-layouts: 2.65 us -> 0.01 us
    pallas_call x1, Pallas kernels: 142 us -> 132 us  [shards(): pl.pallas_call(functools.partial(moe_kernel, num_ep), out_shape=jax.Shape...]
    unnamed x2 -> x4, local copies, waits for them, and re-layouts: 2.34 us -> 0.01 us
where the time goes in v4:
time: 134 us
  Pallas kernels  132 us (99%)
  other arithmetic  1.63 us (1%)
    pallas_call x1, Pallas kernels, shards(): pl.pallas_call(functools.partial(moe_kernel, num_ep), out_shape=jax.Shape...  132 us

profile of v4, /device:TPU:37, one launch (start us, length us, event | category | flops | bytes accessed | tf_op | source)
XLA Modules:
  0.0 133.9 jit_solution(5502207180663185724)
XLA Ops:
  0.0 0.0 copy-start
  0.0 0.0 copy-start.1
  0.0 132.2 %shard_map.82 = f32[64,1024]{1,0:T(8,128)} custom-call(bf16[64,2048]{1,0:T(8,128)(2,1)} %tokens.1, s32[4,64]{1,0:T(4,128)} %bitcast.2, f32[4,64]{1,0:T(4,128)} %bitcast.3, bf16[1,2048,640]{2,1,0:T(8,128)(2,1)} %w_gate.1, bf16[1,2048,640]{2,1,0:T(8,128)(2,1)} %w_up.1, bf16[1,640,2048]{2,1,0:T(8,128)(2,1)} %w_down.1), custom_call_target="tpu_custom_call" | custom-call | tf_op jit(solution)/shard_map/pallas_call | solution.py:344
  132.2 0.0 copy-done
  132.2 0.0 copy-done.1
  132.3 1.6 %add_convert_fusion = bf16[64,1024]{1,0:T(8,128)(2,1)} fusion(f32[64,1024]{1,0:T(8,128)} %shard_map.82, f32[1024]{0:T(1024)S(1)} %copy-done, f32[1024]{0:T(1024)S(1)} %copy-done.1), kind=kLoop, calls=%fused_computation | loop fusion | flops 196608 | bytes 401408 | tf_op jit(solution)/shard_map/convert_element_type | solution.py:377
Async XLA Ops:
  0.0 132.2 %copy-start = (f32[1024]{0:T(1024)S(1)}, f32[1024]{0:T(1024)}, u32[]{:S(2)}) copy-start(f32[1024]{0:T(1024)} %param.15) | copy-start | bytes 12292
  0.0 132.2 %copy-start.1 = (f32[1024]{0:T(1024)S(1)}, f32[1024]{0:T(1024)}, u32[]{:S(2)}) copy-start(f32[1024]{0:T(1024)} %param.14) | copy-start | bytes 12292

commit v5 on v4

--- a/solution.py
+++ b/solution.py
@@ -239,12 +239,9 @@
 
     weight_column(last)
 
-    @pl.loop(0, ff_tiles)
-    def _(j):
+    for j in range(ff_tiles):
         gate_up(last, j)
-
-    @pl.loop(0, chunks)
-    def _(g):
+    for g in range(chunks):
         down(last, g)
         chain[g, slot_rows(hops), :] = sums[g, slot_rows(hops - shift), :].astype(bf16)
         combine_copy(hops, g).start()

time: 134 us -> 133 us (level)
  no operation moved by 1% of the time
where the time goes in v5:
time: 133 us
  Pallas kernels  131 us (98%)
  other arithmetic  1.63 us (1%)
    pallas_call x1, Pallas kernels, shards(): pl.pallas_call(functools.partial(moe_kernel, num_ep), out_shape=jax.Shape...  131 us

profile of v5, /device:TPU:37, one launch (start us, length us, event | category | flops | bytes accessed | tf_op | source)
XLA Modules:
  0.0 132.8 jit_solution(7048641860041612609)
XLA Ops:
  0.0 0.0 copy-start
  0.0 0.0 copy-start.1
  0.0 131.1 %shard_map.82 = f32[64,1024]{1,0:T(8,128)} custom-call(bf16[64,2048]{1,0:T(8,128)(2,1)} %tokens.1, s32[4,64]{1,0:T(4,128)} %bitcast.2, f32[4,64]{1,0:T(4,128)} %bitcast.3, bf16[1,2048,640]{2,1,0:T(8,128)(2,1)} %w_gate.1, bf16[1,2048,640]{2,1,0:T(8,128)(2,1)} %w_up.1, bf16[1,640,2048]{2,1,0:T(8,128)(2,1)} %w_down.1), custom_call_target="tpu_custom_call" | custom-call | tf_op jit(solution)/shard_map/pallas_call | solution.py:341
  131.1 0.0 copy-done
  131.2 0.0 copy-done.1
  131.2 1.6 %add_convert_fusion = bf16[64,1024]{1,0:T(8,128)(2,1)} fusion(f32[64,1024]{1,0:T(8,128)} %shard_map.82, f32[1024]{0:T(1024)S(1)} %copy-done, f32[1024]{0:T(1024)S(1)} %copy-done.1), kind=kLoop, calls=%fused_computation | loop fusion | flops 196608 | bytes 401408 | tf_op jit(solution)/shard_map/convert_element_type | solution.py:374
Async XLA Ops:
  0.0 131.1 %copy-start = (f32[1024]{0:T(1024)S(1)}, f32[1024]{0:T(1024)}, u32[]{:S(2)}) copy-start(f32[1024]{0:T(1024)} %param.15) | copy-start | bytes 12292
  0.0 131.2 %copy-start.1 = (f32[1024]{0:T(1024)S(1)}, f32[1024]{0:T(1024)}, u32[]{:S(2)}) copy-start(f32[1024]{0:T(1024)} %param.14) | copy-start | bytes 12292
